TPU v7x, 512 devices: a 8x2x16 block of a 8x8x16 slice. The times are simulated.
512 devices in a mesh: grp: 2 (over y), fs: 32 (over z, core), tp: 8 (over x).
Axes of the slice: x: 8, y: 2, z: 16, core: 2. Of those that a mesh axis runs over, the one named last changes fastest.
The devices are a block of a 8x8x16 slice.
Arguments:
- tokens: bfloat16 [32768, 2048], P(('grp', 'fs', 'tp')), parts along dimension 0, may hold values from -30 to 30
- gate_master: float32 [2048, 2752], P('fs', 'tp'), may hold values from -0.125 to 0.125
- up_master: float32 [2048, 2752], P('fs', 'tp'), may hold values from -0.125 to 0.125
- down_master: float32 [2048, 2752], P('fs', 'tp'), may hold values from -0.4375 to 0.4375
- norm_gain: float32 [2048], replicated, may hold values from 0.1 to 1.9
- post_gain: float32 [2048], replicated, may hold values from 0.1 to 1.9
- post_bias: float32 [2048], replicated, may hold values from -3 to 3
Outputs:
- gate_ready: bfloat16 [4096, 2752], P('grp', 'tp'), parts along dimension 0
- up_ready: bfloat16 [4096, 2752], P('grp', 'tp'), parts along dimension 0
- down_ready: bfloat16 [4096, 2752], P('grp', 'tp'), parts along dimension 0
- result: bfloat16 [32768, 2048], P(('grp', 'fs', 'tp')), parts along dimension 0
There are 2 independent parts, one for each index of `grp`. A program takes and returns all parts, laid end to end along the dimension named above; an argument that names none is the same for every part. Nothing has to cross between parts.
All inputs are finite; a program needn't handle non-finite values.
Results may differ from a plain program's by a relative error of at most 0.009.
Values may be sent and summed in bfloat16 or wider, within the bound.
A program may use at most 64 MiB of HBM per device.

v0:
```python
import jax
import jax.numpy as jnp
from jax import lax
from jax.sharding import PartitionSpec as P


def sent_together(arrays, axis, dim, along):
    widths = [a.shape[along] for a in arrays]
    both = jnp.concatenate(arrays, axis=along)
    whole = lax.all_gather(both, axis, axis=dim, tiled=True)
    return tuple(jnp.split(whole, [sum(widths[:k]) for k in range(1, len(widths))], axis=along))


def copy_for_each(value, axis):
    devices = lax.axis_size(axis)
    return lax.all_to_all(
        jnp.broadcast_to(value[None], (devices, *value.shape)), axis, 0, 0, tiled=True
    )


def in_order(parts, dim):
    shape = list(parts.shape[1:])
    shape[dim] *= parts.shape[0]
    return jnp.moveaxis(parts, 0, dim).reshape(shape)


def collect(value, axis, dim):
    parts = copy_for_each(value, axis)
    return in_order(parts, dim)


def finish(wide, branch, post_gain, post_bias):
    mixed = jnp.sqrt(jnp.float32(2.0)) * wide + 0.5 * branch
    center = jnp.mean(mixed, axis=-1, keepdims=True)
    spread = jnp.mean(jnp.square(mixed - center), axis=-1, keepdims=True)
    return ((mixed - center) * lax.rsqrt(spread + 1e-05) * post_gain + post_bias).astype(
        jnp.bfloat16
    )


def local(tokens, gate_master, up_master, down_master, norm_gain, post_gain, post_bias):
    row_count = gate_master.shape[0]
    first_row = lax.axis_index("fs") * row_count
    gain_rows = lax.dynamic_slice_in_dim(norm_gain, first_row, row_count, 0)
    gate_piece = (gain_rows[:, None] * gate_master).astype(jnp.bfloat16)
    up_piece = (gain_rows[:, None] * up_master).astype(jnp.bfloat16)
    down_piece = down_master.astype(jnp.bfloat16)
    gate_ready, up_ready, down_ready = sent_together((gate_piece, up_piece, down_piece), "fs", 0, 1)
    wide = tokens.astype(jnp.float32)
    normed = (wide * lax.rsqrt(jnp.mean(wide * wide, axis=-1, keepdims=True) + 1e-06)).astype(
        jnp.bfloat16
    )
    piece = collect(normed, "tp", 0)
    gate = jnp.dot(piece, gate_ready, preferred_element_type=jnp.float32)
    upward = jnp.dot(piece, up_ready, preferred_element_type=jnp.float32)
    hidden = (jax.nn.silu(gate) * upward).astype(jnp.bfloat16)
    branch = lax.psum_scatter(
        lax.dot_general(
            hidden, down_ready, (((1,), (1,)), ((), ())), preferred_element_type=jnp.float32
        ).astype(jnp.bfloat16),
        "tp",
        scatter_dimension=0,
        tiled=True,
    ).astype(jnp.float32)
    result = finish(wide, branch, post_gain, post_bias)
    return (gate_ready, up_ready, down_ready, result)


def solution(mesh):
    return jax.shard_map(
        local,
        mesh=mesh,
        in_specs=(
            P(("grp", "fs", "tp"), None),
            P("fs", "tp"),
            P("fs", "tp"),
            P("fs", "tp"),
            P(),
            P(),
            P(),
        ),
        out_specs=(P("grp", "tp"), P("grp", "tp"), P("grp", "tp"), P(("grp", "fs", "tp"), None)),
        check_vma=False,
    )
```

profile of v0, /device:TPU:65, one launch (start us, length us, event | category | flops | bytes accessed | tf_op | source)
XLA Modules:
  0.0 183.0 jit_solution(13053478238345671993)
XLA Ops:
  7.2 0.1 all-gather.2.cloned.1.call-start
  7.3 0.9 convert_element_type.29
  8.2 0.8 dynamic_slice.3
  8.9 1.0 multiply_convert_fusion
  9.9 0.8 concatenate.3
  10.7 0.1 all-gather.2.cloned.1.call-update
  10.8 0.1 reduce-scatter.2.cloned.1.call-start
  10.9 1.1 fusion.7
  12.0 1.1 fusion.8
  13.1 0.2 broadcast_in_dim.2
  13.3 36.6 %all_to_all.5 = bf16[8,64,2048]{2,1,0:T(8,128)(2,1)S(1)} all-to-all(bf16[8,64,2048]{2,1,0:T(8,128)(2,1)S(1)} %broadcast_in_dim.2), channel_id=1, replica_groups=mesh['grp'=2,'fs'=32,'tp'=8] {'tp'}, dimensions={0} | all-to-all | bytes 4194304 | tf_op jit(solution)/shard_map/all_to_all | solution.py:16
  50.0 72.5 %all-gather.2.cloned.1.call-done = bf16[2048,1032]{1,0:T(8,128)(2,1)} async-done(((bf16[64,1032]{1,0:T(8,128)(2,1)}), bf16[2048,1032]{1,0:T(8,128)(2,1)}) %all-gather.2.cloned.1.call-update) | async-done | bytes 4227088 | tf_op jit(solution)/shard_map/all_gather | solution.py:10
  122.4 2.3 %fusion.15 = f32[512,344]{0,1:T(8,128)S(1)} fusion(bf16[512,2048]{1,0:T(8,128)(2,1)S(1)} %bitcast.3, bf16[2048,1032]{1,0:T(8,128)(2,1)} %all-gather.2.cloned.1.call-done), kind=kOutput, calls=%fused_computation.26 | convolution fusion | flops 721420288 | bytes 4374528 | tf_op jit(solution)/shard_map/dot_general | solution.py:54
  124.8 6.7 %convolution_convert_fusion = bf16[512,2048]{1,0:T(8,128)(2,1)} fusion(bf16[512,2048]{1,0:T(8,128)(2,1)S(1)} %bitcast.4, f32[512,344]{0,1:T(8,128)S(1)} %fusion.15, bf16[2048,1032]{1,0:T(8,128)(2,1)} %all-gather.2.cloned.1.call-done), kind=kOutput, calls=%fused_computation | convolution fusion | flops 1444945920 | bytes 8044544 | tf_op jit(solution)/shard_map/dot_general | solution.py:58
  131.5 0.1 reduce-scatter.2.cloned.1.call-update
  131.6 5.8 %fusion.17 = (bf16[2048,344]{1,0:T(8,128)(2,1)S(1)}, bf16[2048,344]{1,0:T(8,128)(2,1)S(1)}, bf16[2048,344]{1,0:T(8,128)(2,1)}) fusion(bf16[2048,1032]{1,0:T(8,128)(2,1)} %all-gather.2.cloned.1.call-done), kind=kLoop, calls=%fused_computation.28 | loop fusion | bytes 8454144 | tf_op jit(solution)/shard_map/split | solution.py:11
  137.3 2.5 %copy.14 = bf16[2048,344]{0,1:T(8,128)(2,1)} copy(bf16[2048,344]{1,0:T(8,128)(2,1)} %get-tuple-element.10) | data formatting | bytes 2818048
  139.9 1.6 copy.15
  141.4 0.0 copy-start
  141.4 0.0 copy-start.1
  141.4 0.0 copy-start.2
  141.4 1.6 copy.16
  143.0 28.9 %reduce-scatter.2.cloned.1.call-done = bf16[64,2048]{1,0:T(8,128)(2,1)} async-done(((bf16[512,2048]{1,0:T(8,128)(2,1)}), bf16[64,2048]{1,0:T(8,128)(2,1)}) %reduce-scatter.2.cloned.1.call-update) | async-done | bytes 262160 | tf_op jit(solution)/shard_map/reduce_scatter | solution.py:57
  171.9 0.0 copy-done
  171.9 1.2 fusion.10
  173.1 1.2 multiply_reduce_fusion
  174.3 0.0 copy-done.1
  174.3 0.0 copy-done.2
  174.3 1.8 %add_convert_fusion = bf16[64,2048]{1,0:T(8,128)(2,1)} fusion(bf16[64,2048]{1,0:T(8,128)(2,1)} %reduce-scatter.2.cloned.1.call-done, bf16[64,2048]{1,0:T(8,128)(2,1)S(1)} %copy-done, f32[2048]{0:T(1024)S(1)} %copy-done.1, f32[2048]{0:T(1024)S(1)} %copy-done.2, f32[64]{0:T(128)S(1)} %add_rsqrt_fusion, f32[64]{0:T(128)S(1)} %broadcast_multiply_fusion), kind=kLoop, calls=%fused_computation.14 | loop fusion | flops 1310720 | bytes 803328 | tf_op jit(solution)/shard_map/convert_element_type | solution.py:36
  (3 shorter events, 0.0 us)
Async XLA Ops:
  7.2 115.2 %all-gather.2.cloned.1.call-start = ((), (), s32[]{:S(2)}) async-start(), calls=%async_computation.2 | async-start | bytes 4866048 | tf_op jit(solution)/shard_map/all_gather | solution.py:10
  10.8 161.1 %reduce-scatter.2.cloned.1.call-start = ((), (), s32[]{:S(2)}) async-start(), calls=%async_computation.3 | async-start | bytes 2359296 | tf_op jit(solution)/shard_map/reduce_scatter | solution.py:57
  141.4 30.5 %copy-start = (bf16[64,2048]{1,0:T(8,128)(2,1)S(1)}, bf16[64,2048]{1,0:T(8,128)(2,1)}, u32[]{:S(2)}) copy-start(bf16[64,2048]{1,0:T(8,128)(2,1)} %param.7) | copy-start | bytes 786436
  141.4 32.8 %copy-start.1 = (f32[2048]{0:T(1024)S(1)}, f32[2048]{0:T(1024)}, u32[]{:S(2)}) copy-start(f32[2048]{0:T(1024)} %param.13) | copy-start | bytes 24580
  141.4 32.9 %copy-start.2 = (f32[2048]{0:T(1024)S(1)}, f32[2048]{0:T(1024)}, u32[]{:S(2)}) copy-start(f32[2048]{0:T(1024)} %param.12) | copy-start | bytes 24580
Sparse Core Ops, SparseCore 0:
  10.9 111.4 all-gather.1
  131.7 40.1 reduce-scatter.1
where the time goes:
time: 187 us; the launch traced here: 183 us
  waiting for transfers between devices  101 us (54%)
  blocking collectives  36.6 us (20%)
  between operations  14.1 us (8%)
  local copies, waits for them, and re-layouts  13.2 us (7%)
  matrix products  9.08 us (5%)
  other arithmetic  8.29 us (4%)
    all_gather x1, waiting for transfers between devices, sent_together(): whole = lax.all_gather(both, axis, axis=dim, tiled=True)  72.5 us
    all_to_all x1, blocking collectives, copy_for_each(): lax.all_to_all(jnp.broadcast_to(value[None], (devices, *value.shape)), ax...  36.6 us
    reduce_scatter x1, waiting for transfers between devices, local(): lax.psum_scatter(lax.dot_general(hidden, down_ready, (((1,), (1,)), ((),...  28.9 us
    dot_general x1, matrix products, local(): lax.dot_general(hidden, down_ready, (((1,), (1,)), ((), ())), preferred_e...  6.74 us
    split x1, local copies, waits for them, and re-layouts, sent_together(): jnp.split(whole, [sum(widths[:k]) for k in range(1, len(widths))], axis=a...  5.77 us
    unnamed x9, local copies, waits for them, and re-layouts  5.68 us
  transfers between devices with their start and end apart: 2, of which 2 were waited for; matrix products, arithmetic and copies ran while one was open for 8% of the time, Pallas kernels for 0%

commit v1 on v0

v1 whole, which is shorter than its diff:
```python
import functools

import jax
import jax.numpy as jnp
from jax import lax
from jax.experimental import pallas as pl
from jax.experimental.pallas import tpu as pltpu
from jax.sharding import PartitionSpec as P

MESH = pl.DeviceIdType.MESH
CUTS = 4
VMEM_SPACE = pl.BlockSpec(memory_space=pltpu.VMEM)
ANY_SPACE = pl.BlockSpec(memory_space=pl.ANY)


def rows_of(index, size):
    return pl.ds(pl.multiple_of(index * size, size), size)


def gather_and_reduce(
    n_fs, n_tp, tokens, gate, up, down, gain, ready, branch,
    tok_in, w_in, normed, hidden, partial, sent, landed,
    in_sem, z_recv, z_send, core_recv, core_send, x_recv, x_send, r_recv, r_send,
):
    f, t = lax.axis_index("fs"), lax.axis_index("tp")
    block, width = tok_in.shape
    piece = w_in.shape[1]
    far_z, far_x = n_fs // 4, n_tp // 2
    side = width // 2
    cut = side // CUTS

    loads = [pltpu.make_async_copy(tokens, tok_in, in_sem.at[0])]
    for m, master in enumerate((gate, up, down)):
        loads.append(pltpu.make_async_copy(master, w_in.at[m], in_sem.at[1 + m]))
    for load in loads:
        load.start()

    z_next = (lax.rem(f + 2, n_fs), lax.rem(f + n_fs - 2, n_fs))
    x_next = (lax.rem(t + 1, n_tp), lax.rem(t + n_tp - 1, n_tp))
    other = f + 1 - 2 * lax.rem(f, 2)
    barrier = pltpu.get_barrier_semaphore()
    for there in ({"fs": z_next[0]}, {"fs": z_next[1]}, {"fs": other}, {"tp": x_next[0]}, {"tp": x_next[1]}):
        pl.semaphore_signal(barrier, inc=1, device_id=there, device_id_type=MESH)

    gain_row = gain[pl.ds(f // 2, 1), :]
    lane = lax.broadcasted_iota(jnp.int32, (piece, gain_row.shape[1]), 1)
    row = lax.broadcasted_iota(jnp.int32, (piece, gain_row.shape[1]), 0)
    gain_col = jnp.sum(
        jnp.where(lane == row + lax.rem(f, 2) * piece, gain_row, 0.0), axis=1, keepdims=True
    )
    own = rows_of(f, piece)
    for m in range(3):
        loads[1 + m].wait()
        value = w_in[m]
        if m < 2:
            value = gain_col * value
        ready[m, own, :] = value.astype(jnp.bfloat16)
    loads[0].wait()
    wide = tok_in[...].astype(jnp.float32)
    own_slot = (n_tp - 1) * block
    normed[pl.ds(own_slot, block), :] = (
        wide * lax.rsqrt(jnp.mean(wide * wide, axis=-1, keepdims=True) + 1e-06)
    ).astype(jnp.bfloat16)
    pl.semaphore_wait(barrier, 5)

    def z_rows(d, k):
        away = 2 * k if d == 0 else n_fs - 2 * k
        start = lax.rem(f + n_fs - away, n_fs) * piece
        if k < far_z:
            return pl.ds(pl.multiple_of(start, piece), piece)
        start = start + d * (piece // 2)
        return pl.ds(pl.multiple_of(start, piece // 2), piece // 2)

    def z_copy(d, k, m):
        rows = z_rows(d, k - 1) if k < far_z else None
        if rows is None:
            away = 2 * (k - 1) if d == 0 else n_fs - 2 * (k - 1)
            start = lax.rem(f + n_fs - away, n_fs) * piece + d * (piece // 2)
            rows = pl.ds(pl.multiple_of(start, piece // 2), piece // 2)
        ref = ready.at[m, rows, :]
        return pltpu.make_async_remote_copy(
            src_ref=ref, dst_ref=ref, send_sem=z_send.at[d, m], recv_sem=z_recv.at[d, k - 1, m],
            device_id={"fs": z_next[d]}, device_id_type=MESH,
        )

    def core_copy(rows, m):
        ref = ready.at[m, rows, :]
        return pltpu.make_async_remote_copy(
            src_ref=ref, dst_ref=ref, send_sem=core_send.at[m], recv_sem=core_recv.at[m],
            device_id={"fs": other}, device_id_type=MESH,
        )

    half = block // 2

    def slot(d, k):
        if k == 0:
            return own_slot
        return (2 * (k - 1) + (d if k < far_x else 0)) * block

    def x_copy(d, k, h):
        src = normed.at[pl.ds(slot(d, k - 1) + h * half, half), :]
        dst = normed.at[pl.ds(slot(d, k) + h * half, half), :]
        return pltpu.make_async_remote_copy(
            src_ref=src, dst_ref=dst, send_sem=x_send.at[d], recv_sem=x_recv.at[d, k - 1, h],
            device_id={"tp": x_next[d]}, device_id_type=MESH,
        )

    for d in range(2):
        for m in range(3):
            z_copy(d, 1, m).start()
        for h in range(2):
            x_copy(d, 1, h).start()
    for m in range(3):
        core_copy(own, m).start()

    events = []
    for k in range(1, far_z + 1):
        for m in range(3):
            size = 1.0 if k < far_z else 0.5
            events.append((1.9 + 3.15 * (k - 1) + 1.05 * size * (m + 1), "z", k, m))
    for k in range(1, far_x + 1):
        for h in range(2):
            events.append((1.9 + 5.6 * (k - 1) + 2.8 * (h + 1), "x", k, h))
    for _, kind, k, i in sorted(events):
        for d in range(2):
            if kind == "z":
                z_copy(d, k, i).wait_recv()
                if k < far_z:
                    z_copy(d, k + 1, i).start()
                core_copy(z_rows(d, k), i).start()
            else:
                if k == far_x and i != d:
                    continue
                x_copy(d, k, i).wait_recv()
                if k + 1 < far_x or (k + 1 == far_x and i == d):
                    x_copy(d, k + 1, i).start()
    for m in range(3):
        pltpu.make_async_copy(
            ready.at[m, pl.ds(0, n_fs // 2 * piece), :],
            ready.at[m, pl.ds(0, n_fs // 2 * piece), :],
            core_recv.at[m],
        ).wait()

    def compute(pair):
        rows = pl.ds(pair * 2 * block, 2 * block)
        x = normed[rows, :]
        g = jnp.dot(x, ready[0], preferred_element_type=jnp.float32)
        u = jnp.dot(x, ready[1], preferred_element_type=jnp.float32)
        hidden[rows, :] = (g * (1.0 / (1.0 + jnp.exp(-g))) * u).astype(jnp.bfloat16)
        h = hidden[rows, :]
        for j in range(width // cut):
            partial[j, rows, :] = lax.dot_general(
                h, ready[2, pl.ds(j * cut, cut), :], (((1,), (1,)), ((), ())),
                preferred_element_type=jnp.float32,
            ).astype(jnp.bfloat16)

    def r_copy(d, s, j):
        return pltpu.make_async_remote_copy(
            src_ref=sent.at[d, s, j], dst_ref=landed.at[d, s, j],
            send_sem=r_send.at[d], recv_sem=r_recv.at[d, s, j],
            device_id={"tp": x_next[d]}, device_id_type=MESH,
        )

    def r_slot(d, s):
        k = s + 1
        if k == n_tp:
            return own_slot
        return slot(d, k) if k <= far_x else slot(1 - d, n_tp - k)

    pairs = n_tp // 2
    for s in range(n_tp):
        if s < pairs:
            compute(s)
        for j in range(CUTS):
            for d in range(2):
                mine = partial[d * CUTS + j, pl.ds(r_slot(d, s), block), :].astype(jnp.float32)
                if s > 0:
                    r_copy(d, s - 1, j).wait_recv()
                    mine = mine + landed[d, s - 1, j].astype(jnp.float32)
                if s < n_tp - 1:
                    sent[d, s, j] = mine.astype(jnp.bfloat16)
                    r_copy(d, s, j).start()
                else:
                    branch[:, pl.ds(d * side + j * cut, cut)] = mine

    gone = pl.ds(0, (2 * far_z - 1) * piece // 2)
    for m in range(3):
        for d in range(2):
            pltpu.make_async_copy(ready.at[m, gone, :], ready.at[m, gone, :], z_send.at[d, m]).wait()
        pltpu.make_async_copy(
            ready.at[m, pl.ds(0, n_fs // 2 * piece), :],
            ready.at[m, pl.ds(0, n_fs // 2 * piece), :],
            core_send.at[m],
        ).wait()
    gone = pl.ds(0, (2 * far_x - 1) * half)
    for d in range(2):
        pltpu.make_async_copy(normed.at[gone, :], normed.at[gone, :], x_send.at[d]).wait()
        pltpu.make_async_copy(sent.at[d], sent.at[d], r_send.at[d]).wait()


def finish(ready, branch, tokens, post_gain, post_bias, gate, up, down, result, sem):
    for m, out in enumerate((gate, up, down)):
        pltpu.make_async_copy(ready.at[m], out, sem.at[m]).start()
    mixed = jnp.sqrt(jnp.float32(2.0)) * tokens[...].astype(jnp.float32) + 0.5 * branch[...]
    center = jnp.mean(mixed, axis=-1, keepdims=True)
    off = mixed - center
    spread = jnp.mean(jnp.square(off), axis=-1, keepdims=True)
    result[...] = (off * lax.rsqrt(spread + 1e-05) * post_gain[...] + post_bias[...]).astype(jnp.bfloat16)
    for m, out in enumerate((gate, up, down)):
        pltpu.make_async_copy(ready.at[m], out, sem.at[m]).wait()


def local(n_fs, n_tp, tokens, gate, up, down, norm_gain, post_gain, post_bias):
    block, width = tokens.shape
    piece, units = gate.shape
    far_z, far_x = n_fs // 4, n_tp // 2
    whole = n_fs * piece
    cut = width // 2 // CUTS
    steps = n_tp - 1
    bf16, f32 = jnp.bfloat16, jnp.float32
    dma = pltpu.SemaphoreType.DMA
    ready, branch = pl.pallas_call(
        functools.partial(gather_and_reduce, n_fs, n_tp),
        out_shape=(
            pltpu.VMEM((3, whole, units), bf16),
            pltpu.VMEM((block, width), f32),
        ),
        in_specs=[ANY_SPACE] * 4 + [VMEM_SPACE],
        out_specs=(VMEM_SPACE, VMEM_SPACE),
        scratch_shapes=[
            pltpu.VMEM((block, width), bf16),
            pltpu.VMEM((3, piece, units), f32),
            pltpu.VMEM((n_tp * block, width), bf16),
            pltpu.VMEM((n_tp * block, units), bf16),
            pltpu.VMEM((2 * CUTS, n_tp * block, cut), bf16),
            pltpu.VMEM((2, steps, CUTS, block, cut), bf16),
            pltpu.VMEM((2, steps, CUTS, block, cut), bf16),
            dma((4,)),
            dma((2, far_z, 3)),
            dma((2, 3)),
            dma((3,)),
            dma((3,)),
            dma((2, far_x, 2)),
            dma((2,)),
            dma((2, steps, CUTS)),
            dma((2,)),
        ],
        compiler_params=pltpu.CompilerParams(
            collective_id=0, has_side_effects=True, vmem_limit_bytes=40 * 1024 * 1024
        ),
    )(tokens, gate, up, down, norm_gain.reshape(-1, 2 * piece))
    return pl.pallas_call(
        finish,
        out_shape=(
            jax.ShapeDtypeStruct((whole, units), bf16),
            jax.ShapeDtypeStruct((whole, units), bf16),
            jax.ShapeDtypeStruct((whole, units), bf16),
            jax.ShapeDtypeStruct((block, width), bf16),
        ),
        in_specs=[VMEM_SPACE] * 5,
        out_specs=(ANY_SPACE, ANY_SPACE, ANY_SPACE, VMEM_SPACE),
        scratch_shapes=[dma((3,))],
        compiler_params=pltpu.CompilerParams(vmem_limit_bytes=24 * 1024 * 1024),
    )(ready, branch, tokens, post_gain.reshape(1, -1), post_bias.reshape(1, -1))


def solution(mesh):
    return jax.shard_map(
        functools.partial(local, mesh.shape["fs"], mesh.shape["tp"]),
        mesh=mesh,
        in_specs=(
            P(("grp", "fs", "tp"), None),
            P("fs", "tp"),
            P("fs", "tp"),
            P("fs", "tp"),
            P(),
            P(),
            P(),
        ),
        out_specs=(P("grp", "tp"), P("grp", "tp"), P("grp", "tp"), P(("grp", "fs", "tp"), None)),
        check_vma=False,
    )
```

time: 187 us -> 119 us (0.64); the launches traced: 183 us -> 117 us
  Pallas kernels: 0 us -> 104 us
  waiting for transfers between devices: 101 us -> 0 us
  blocking collectives: 36.6 us -> 0 us
  between operations: 14.1 us -> 0.68 us
  matrix products: 9.08 us -> 0 us
  other arithmetic: 8.29 us -> 0 us
    pallas_call x0 -> x2, Pallas kernels: none -> 104 us  [the longest x1 102 us: local(): pl.pallas_call(functools.partial(gather_and_reduce, n_fs, n_tp), out_shap...]
    all_gather x1 -> x0, waiting for transfers between devices: 72.5 us -> none  [sent_together(): whole = lax.all_gather(both, axis, axis=dim, tiled=True)]
    all_to_all x1 -> x0, blocking collectives: 36.6 us -> none  [copy_for_each(): lax.all_to_all(jnp.broadcast_to(value[None], (devices, *value.shape)), ax...]
    reduce_scatter x1 -> x0, waiting for transfers between devices: 28.9 us -> none  [local(): lax.psum_scatter(lax.dot_general(hidden, down_ready, (((1,), (1,)), ((),...]
    dot_general x2 -> x0, matrix products: 9.08 us -> none  [the longest x1 6.74 us: local(): lax.dot_general(hidden, down_ready, (((1,), (1,)), ((), ())), preferred_e...]
    split x1 -> x0, local copies, waits for them, and re-layouts: 5.77 us -> none  [sent_together(): jnp.split(whole, [sum(widths[:k]) for k in range(1, len(widths))], axis=a...]
    pallas_call x0 -> x3, local copies, waits for them, and re-layouts: none -> 5.66 us  [local(): pl.pallas_call(finish, out_shape=(jax.ShapeDtypeStruct((whole, units), bf...]
    convert_element_type x4 -> x0, other arithmetic: 4.83 us -> none  [the longest x1 1.84 us: finish(): ((mixed - center) * lax.rsqrt(spread + 1e-05) * post_gain + post_bias).as...]
  transfers between devices with their start and end apart: 2 -> 0, of which waited for: 2 -> 0; matrix products, arithmetic and copies ran while one was open for 8% -> 0% of each run, Pallas kernels for 0% -> 0%
where the time goes in v1:
time: 119 us; the launch traced here: 117 us
  Pallas kernels  104 us (87%)
  local copies, waits for them, and re-layouts  12.5 us (11%)
    pallas_call x1, Pallas kernels, local(): pl.pallas_call(functools.partial(gather_and_reduce, n_fs, n_tp), out_shap...  102 us
    unnamed x16, local copies, waits for them, and re-layouts  6.84 us
    pallas_call x3, local copies, waits for them, and re-layouts, local(): pl.pallas_call(finish, out_shape=(jax.ShapeDtypeStruct((whole, units), bf...  5.66 us

profile of v1, /device:TPU:65, one launch (start us, length us, event | category | flops | bytes accessed | tf_op | source)
XLA Modules:
  0.0 116.9 jit_solution(18087194210516145812)
XLA Ops:
  0.6 0.0 copy-start.1
  0.6 0.9 copy-done.1
  1.6 0.0 copy-start.2
  1.6 0.9 copy-done.2
  2.5 0.0 copy-start.3
  2.5 0.9 copy-done.3
  3.4 0.0 copy-start.4
  3.4 0.9 copy-done.4
  4.3 0.0 copy-start.5
  4.3 0.7 copy-done.5
  5.0 102.4 %shard_map.102 = (bf16[3,2048,344]{2,1,0:T(8,128)(2,1)S(1)}, f32[64,2048]{1,0:T(8,128)S(1)}) custom-call(bf16[64,2048]{1,0:T(8,128)(2,1)S(1)} %copy-done.1, f32[64,344]{1,0:T(8,128)S(1)} %copy-done.2, f32[64,344]{1,0:T(8,128)S(1)} %copy-done.3, f32[64,344]{1,0:T(8,128)S(1)} %copy-done.4, f32[16,128]{1,0:T(8,128)S(1)} %bitcast.3), custom_call_target="tpu_custom_call" | custom-call | tf_op jit(solution)/shard_map/pallas_call | solution.py:222
  107.3 0.0 copy-start.6
  107.4 0.7 copy-done.6
  108.0 0.0 copy-start.7
  108.0 0.7 copy-done.7
  108.7 1.3 %shard_map.103 = (bf16[2048,344]{1,0:T(8,128)(2,1)S(1)}, bf16[2048,344]{1,0:T(8,128)(2,1)S(1)}, bf16[2048,344]{1,0:T(8,128)(2,1)S(1)}, bf16[64,2048]{1,0:T(8,128)(2,1)}) custom-call(bf16[3,2048,344]{2,1,0:T(8,128)(2,1)S(1)} %get-tuple-element.6.ready, f32[64,2048]{1,0:T(8,128)S(1)} %get-tuple-element.7.branch, bf16[64,2048]{1,0:T(8,128)(2,1)S(1)} %copy-done.1, ...), custom_call_target="tpu_custom_call" | custom-call | tf_op jit(solution)/shard_map/pallas_call | solution.py:252
  110.1 0.0 copy-start
  110.1 1.1 copy-done
  111.2 2.5 %copy.11 = bf16[2048,344]{0,1:T(8,128)(2,1)} copy(bf16[2048,344]{1,0:T(8,128)(2,1)} %copy-done) | data formatting | bytes 2818048 | tf_op jit(solution)/shard_map/pallas_call | solution.py:252
  113.8 1.6 %copy.12 = bf16[2048,344]{0,1:T(8,128)(2,1)} copy(bf16[2048,344]{1,0:T(8,128)(2,1)S(1)} %get-tuple-element.9) | data formatting | bytes 2818048 | tf_op jit(solution)/shard_map/pallas_call | solution.py:252
  115.3 1.6 %copy.13 = bf16[2048,344]{0,1:T(8,128)(2,1)} copy(bf16[2048,344]{1,0:T(8,128)(2,1)S(1)} %get-tuple-element.10) | data formatting | bytes 2818048 | tf_op jit(solution)/shard_map/pallas_call | solution.py:252
Async XLA Ops:
  0.6 1.0 copy-start.1
  1.6 0.9 copy-start.2
  2.5 0.9 copy-start.3
  3.4 0.9 copy-start.4
  4.3 0.7 copy-start.5
  107.3 0.7 copy-start.6
  108.0 0.7 copy-start.7
  110.1 1.1 copy-start

commit v2 on v0

v2 whole, which is shorter than its diff:
```python
import functools

import jax
import jax.numpy as jnp
from jax import lax
from jax.experimental import pallas as pl
from jax.experimental.pallas import tpu as pltpu
from jax.sharding import PartitionSpec as P

MESH = pl.DeviceIdType.MESH
CUTS = 8
TOP = 8
PARTS = 3
VMEM_SPACE = pl.BlockSpec(memory_space=pltpu.VMEM)
HBM_SPACE = pl.BlockSpec(memory_space=pltpu.HBM)


def gather_and_reduce(
    n_fs, n_tp, units, tokens, gate, up, down, gain, post_gain, post_bias, ready, mixed, affine,
    tok_in, w_in, gain_in, normed, partial, sent, landed,
    in_sem, swap_sem, a_recv, a_send, b_recv, b_send, c_recv, c_send, core_recv, core_send,
    x_recv, x_send, r_recv, r_send, first_in,
):
    f, t = lax.axis_index("fs"), lax.axis_index("tp")
    nz = n_fs // 2
    z, c = f // 2, lax.rem(f, 2)
    low = nz - TOP
    block, width = tok_in.shape
    piece = w_in.shape[1] // 2
    pair_cols = 2 * piece
    share = ready.shape[2] // 2
    far = n_tp // 2
    cut = width // CUTS
    other = f + 1 - 2 * c

    def remote(src, dst, send, recv, **there):
        return pltpu.make_async_remote_copy(
            src_ref=src, dst_ref=dst, send_sem=send, recv_sem=recv,
            device_id=there, device_id_type=MESH,
        )

    def near(step):
        return lax.rem(t + step + n_tp, n_tp)

    barrier = pltpu.get_barrier_semaphore()

    def greet(**there):
        pl.semaphore_signal(barrier, inc=1, device_id=there, device_id_type=MESH)

    greet(fs=other)
    for step in (1, -1, 2, -2):
        greet(tp=near(step))

    @pl.when(z > 0)
    def _():
        greet(fs=f - 2)

    @pl.when((z > 0) & (z < nz - 1))
    def _():
        greet(fs=f + 2)

    @pl.when(z == 0)
    def _():
        for i in range(TOP):
            greet(fs=c + 2 * (low + i))

    my_rows = pl.ds(pl.multiple_of(c * piece, piece), piece)
    masters = (gate, up, down)
    loads = [pltpu.make_async_copy(tokens, tok_in, in_sem.at[0])]
    loads.append(pltpu.make_async_copy(gain.at[pl.ds(z, 1), :], gain_in, in_sem.at[1]))
    for m in range(3):
        loads.append(pltpu.make_async_copy(masters[m], w_in.at[m, my_rows, :], in_sem.at[2 + m]))
    loads.append(pltpu.make_async_copy(post_gain, affine.at[0], in_sem.at[5]))
    loads.append(pltpu.make_async_copy(post_bias, affine.at[1], in_sem.at[6]))
    for load in loads:
        load.start()

    count = 5 + jnp.where(z > 1, 1, 0) + jnp.where(z < nz - 1, 1, 0) + jnp.where(z >= low, 1, 0)
    pl.semaphore_wait(barrier, count)

    @pl.when(z == 0)
    def _():
        pl.semaphore_signal(first_in, inc=1, device_id={"fs": f + 2}, device_id_type=MESH)

    swaps = []
    for m in range(3):
        swaps.append(remote(masters[m], w_in.at[m, my_rows, :], swap_sem.at[0, m], swap_sem.at[1, m], fs=other))
        swaps[m].start()

    own_slot = (n_tp - 1) * block

    def slot(d, k):
        if k == 0:
            return own_slot
        return (2 * (k - 1) + (d if k < far else 0)) * block

    half = block // 2

    def x_copy(d, k_from, k_to):
        size = half if k_to == far else block
        shift = d * half if k_to == far else 0
        step = k_to - k_from
        return remote(
            normed.at[pl.ds(slot(d, k_from) + shift, size), :],
            normed.at[pl.ds(slot(d, k_to) + shift, size), :],
            x_send.at[d], x_recv.at[d, k_to - 1], tp=near(step if d == 0 else -step),
        )

    loads[1].wait()
    lane = lax.broadcasted_iota(jnp.int32, (pair_cols, pair_cols), 1)
    row = lax.broadcasted_iota(jnp.int32, (pair_cols, pair_cols), 0)
    gain_col = jnp.sum(jnp.where(lane == row, gain_in[...], 0.0), axis=1, keepdims=True)

    for m in range(3):
        loads[2 + m].wait()
        swaps[m].wait()
        value = w_in[m]
        if m < 2:
            value = gain_col * value
        ready[z, m, pl.ds(0, units), :] = value.T.astype(jnp.bfloat16)
        ready[z, m, pl.ds(units, 2 * share - units), :] = jnp.zeros(
            (2 * share - units, pair_cols), jnp.bfloat16
        )

    def part(i, index):
        if i < 2:
            return ready.at[index, c, pl.ds(i * share, share), :]
        return ready.at[index, 2, pl.ds(pl.multiple_of(c * share, 16), share), :]

    def a_copy(i, j, index):
        ref = part(i, index)
        return remote(ref, ref, a_send.at[j - 1], a_recv.at[j - 1, i], fs=f + 2)

    def b_copy(i, j, index):
        ref = part(i, index)
        return remote(ref, ref, b_send.at[j - 1], b_recv.at[j - 1, i], fs=f - 2)

    def c_copy(i, j, index, there):
        ref = part(i, index)
        return remote(ref, ref, c_send.at[j], c_recv.at[j, i], fs=there)

    def core_copy(i, index):
        ref = part(i, index)
        return remote(ref, ref, core_send.at[i], core_recv.at[i], fs=other)

    goes_right = z < nz - 1
    goes_left = (z > 1) & (z != low)
    passes_top = z < low - 1

    @pl.when(z >= low)
    def _():
        for i in range(PARTS):
            c_copy(i, z - low, z, c).start()

    @pl.when(goes_left)
    def _():
        for i in range(PARTS):
            b_copy(i, 1, z).start()

    @pl.when(goes_right)
    def _():
        for i in range(PARTS):
            a_copy(i, 1, z).start()

    loads[0].wait()
    wide = tok_in[...].astype(jnp.float32)
    normed[pl.ds(own_slot, block), :] = (
        wide * lax.rsqrt(jnp.mean(wide * wide, axis=-1, keepdims=True) + 1e-06)
    ).astype(jnp.bfloat16)
    for k in (2, 1):
        for d in range(2):
            x_copy(d, 0, k).start()

    left_most = max(low, TOP) - 1
    last_left = jnp.where(z < low, low - 1, nz - 1)
    events = []
    for j in range(1, nz - 1):
        events.append((2.0 + 2.83 * j, "a", j))
    for j in range(1, left_most + 1):
        events.append((3.0 + 5.2 * j, "b", j))
    for j in range(TOP):
        events.append((2.0 * low + 18.0 + 2.83 * j, "c", j))
    events.append((16.0, "x", 0))
    events.append((2.0 * low + 17.0, "first", 0))
    events.append((3.1 + 5.2 * (low - 2), "zero", 0))
    for j in range(1, low):
        events.append((1000.0 + j, "end", j))
    for _, kind, j in sorted(events):
        if kind == "x":
            for d in range(2):
                x_copy(d, 0, 2).wait_recv()
                for k in (far, 3):
                    x_copy(d, 2, k).start()
        if kind == "zero":

            @pl.when(z == 1)
            def _():
                pl.semaphore_wait(first_in, 1)
                for q in range(1, low):
                    for i in range(PARTS):
                        b_copy(i, q, q).start()

        if kind == "end":

            @pl.when(z == 0)
            def _():
                for i in range(PARTS):
                    b_copy(i, j, j).wait_recv()
                    core_copy(i, j).start()

        if kind == "first":

            @pl.when(z > 0)
            def _():
                for i in range(PARTS):
                    a_copy(i, z, 0).wait_recv()

                    @pl.when(goes_right)
                    def _():
                        a_copy(i, z + 1, 0).start()

                    core_copy(i, 0).start()

        if kind == "a":

            @pl.when(z > j)
            def _():
                for i in range(PARTS):
                    a_copy(i, j, z - j).wait_recv()

                    @pl.when(goes_right)
                    def _():
                        a_copy(i, j + 1, z - j).start()

                    core_copy(i, z - j).start()

        if kind == "b":

            @pl.when((z > 0) & (z + j <= last_left))
            def _():
                for i in range(PARTS):
                    b_copy(i, j, z + j).wait_recv()

                    @pl.when(goes_left)
                    def _():
                        b_copy(i, j + 1, z + j).start()

                    core_copy(i, z + j).start()

        if kind == "c":

            @pl.when(z < low)
            def _():
                for i in range(PARTS):
                    c_copy(i, j, low + j, c).wait_recv()

                    @pl.when(passes_top)
                    def _():
                        c_copy(i, j, low + j, f + 2).start()

                    core_copy(i, low + j).start()

    all_others = pl.ds(0, nz - 1)
    for i in range(PARTS):
        ref = ready.at[all_others, 0, pl.ds(0, share), :]
        pltpu.make_async_copy(ref, ref, core_recv.at[i]).wait()

    def cut_of(m, j):
        each = cut // pair_cols
        return jnp.concatenate([ready[j * each + i, m, pl.ds(0, units), :] for i in range(each)], axis=1)

    def compute(k):
        for d in range(2):
            if k == far:
                x_copy(d, 2, far).wait_recv()
            elif k != 2:
                x_copy(d, 0 if k == 1 else 2, k).wait_recv()
        rows = pl.ds(slot(0, k), 2 * block)
        dims = (((1,), (1,)), ((), ()))
        g = u = None
        for j in range(CUTS):
            x = normed[rows, pl.ds(j * cut, cut)]
            g_more = lax.dot_general(x, cut_of(0, j), dims, preferred_element_type=jnp.float32)
            u_more = lax.dot_general(x, cut_of(1, j), dims, preferred_element_type=jnp.float32)
            g = g_more if j == 0 else g + g_more
            u = u_more if j == 0 else u + u_more
        h = (g * (1.0 / (1.0 + jnp.exp(-g))) * u).astype(jnp.bfloat16)
        for j in range(CUTS):
            partial[j, rows, :] = jnp.dot(
                h, cut_of(2, j), preferred_element_type=jnp.float32
            ).astype(jnp.bfloat16)

    def r_copy(d, s, j):
        return remote(
            sent.at[d, s, j], landed.at[d, s, j], r_send.at[d, min(s, 1)], r_recv.at[d, s, j],
            tp=near(1 - 2 * d),
        )

    side = CUTS // 2
    for s in range(far):
        k = far - s
        compute(k)
        for at in range(side if s == 0 else CUTS):
            for d in range(2):
                j = d * side + at if s == 0 else ((1 - d) * side + at) % CUTS
                value = partial[j, pl.ds(slot(1 - d, k), block), :]
                if s > 0 and not (s == 1 and j // side != d):
                    r_copy(d, s - 1, j).wait_recv()
                    value = (
                        value.astype(jnp.float32) + landed[d, s - 1, j].astype(jnp.float32)
                    ).astype(jnp.bfloat16)
                sent[d, s, j] = value
                r_copy(d, s, j).start()
    for at in range(CUTS):
        j = at
        value = partial[j, pl.ds(own_slot, block), :].astype(jnp.float32)
        for d in range(2):
            r_copy(d, far - 1, j).wait_recv()
            value = value + landed[d, far - 1, j].astype(jnp.float32)
        cols = pl.ds(j * cut, cut)
        mixed[:, cols] = jnp.sqrt(jnp.float32(2.0)) * tok_in[:, cols].astype(jnp.float32) + 0.5 * value

    loads[5].wait()
    loads[6].wait()

    three = ready.at[pl.ds(0, PARTS), 0, pl.ds(0, share), :]

    def left(sem):
        pltpu.make_async_copy(three, three, sem).wait()

    for j in range(1, nz):

        @pl.when(goes_right & (z >= j - 1))
        def _():
            left(a_send.at[j - 1])

    for j in range(1, left_most + 1):

        @pl.when((goes_left | (z == 1)) & (z + j - 1 <= last_left))
        def _():
            left(b_send.at[j - 1])

    for j in range(TOP):

        @pl.when(passes_top | (z == low + j))
        def _():
            left(c_send.at[j])

    for i in range(PARTS):
        ref = ready.at[all_others, 0, pl.ds(0, share), :]
        pltpu.make_async_copy(ref, ref, core_send.at[i]).wait()
    gone = normed.at[pl.ds(0, 3 * block + half), :]
    for d in range(2):
        pltpu.make_async_copy(gone, gone, x_send.at[d]).wait()
        for ref, at in ((sent.at[d, 0, pl.ds(0, side)], 0), (sent.at[d, pl.ds(1, far - 1)], 1)):
            pltpu.make_async_copy(ref, ref, r_send.at[d, at]).wait()


def finish(units, ready, mixed, affine, gate, up, down, result, put_sem):
    puts = []
    pieces, cols = ready.shape[0], ready.shape[3]
    for m, out in enumerate((gate, up, down)):
        for i in range(pieces):
            puts.append(
                pltpu.make_async_copy(
                    ready.at[i, m, pl.ds(0, units), :], out.at[:, pl.ds(i * cols, cols)], put_sem.at[m, i]
                )
            )
    for put in puts:
        put.start()
    center = jnp.mean(mixed[...], axis=-1, keepdims=True)
    off = mixed[...] - center
    spread = jnp.mean(jnp.square(off), axis=-1, keepdims=True)
    result[...] = (off * lax.rsqrt(spread + 1e-05) * affine[0] + affine[1]).astype(jnp.bfloat16)
    for put in puts:
        put.wait()


def local(n_fs, n_tp, tokens, gate, up, down, norm_gain, post_gain, post_bias):
    block, width = tokens.shape
    piece, units = gate.shape
    nz, far = n_fs // 2, n_tp // 2
    share = -(-units // 32) * 16
    cut = width // CUTS
    bf16, f32 = jnp.bfloat16, jnp.float32
    dma = pltpu.SemaphoreType.DMA
    left_most = max(nz - TOP, TOP) - 1
    ready, mixed, affine = pl.pallas_call(
        functools.partial(gather_and_reduce, n_fs, n_tp, units),
        out_shape=(
            pltpu.VMEM((nz, 3, 2 * share, 2 * piece), bf16),
            pltpu.VMEM((block, width), f32),
            pltpu.VMEM((2, 1, width), f32),
        ),
        in_specs=[HBM_SPACE] * 7,
        out_specs=(VMEM_SPACE, VMEM_SPACE, VMEM_SPACE),
        scratch_shapes=[
            pltpu.VMEM((block, width), bf16),
            pltpu.VMEM((3, 2 * piece, units), f32),
            pltpu.VMEM((1, 2 * piece), f32),
            pltpu.VMEM((n_tp * block, width), bf16),
            pltpu.VMEM((CUTS, n_tp * block, cut), bf16),
            pltpu.VMEM((2, far, CUTS, block, cut), bf16),
            pltpu.VMEM((2, far, CUTS, block, cut), bf16),
            dma((7,)),
            dma((2, 3)),
            dma((nz - 1, PARTS)),
            dma((nz - 1,)),
            dma((left_most, PARTS)),
            dma((left_most,)),
            dma((TOP, PARTS)),
            dma((TOP,)),
            dma((PARTS,)),
            dma((PARTS,)),
            dma((2, far)),
            dma((2,)),
            dma((2, far, CUTS)),
            dma((2, 2)),
            pltpu.SemaphoreType.REGULAR,
        ],
        compiler_params=pltpu.CompilerParams(
            collective_id=0, has_side_effects=True, vmem_limit_bytes=58 * 1024 * 1024
        ),
    )(
        tokens, gate, up, down, norm_gain.reshape(-1, 2 * piece),
        post_gain.reshape(1, -1), post_bias.reshape(1, -1),
    )
    gate_out, up_out, down_out, result = pl.pallas_call(
        functools.partial(finish, units),
        out_shape=(
            pltpu.HBM((units, n_fs * piece), bf16),
            pltpu.HBM((units, n_fs * piece), bf16),
            pltpu.HBM((units, n_fs * piece), bf16),
            jax.ShapeDtypeStruct((block, width), bf16),
        ),
        in_specs=[VMEM_SPACE] * 3,
        out_specs=(HBM_SPACE, HBM_SPACE, HBM_SPACE, VMEM_SPACE),
        scratch_shapes=[dma((3, nz))],
        compiler_params=pltpu.CompilerParams(vmem_limit_bytes=48 * 1024 * 1024),
    )(ready, mixed, affine)
    return gate_out.T, up_out.T, down_out.T, result


def solution(mesh):
    return jax.shard_map(
        functools.partial(local, mesh.shape["fs"], mesh.shape["tp"]),
        mesh=mesh,
        in_specs=(
            P(("grp", "fs", "tp"), None),
            P("fs", "tp"),
            P("fs", "tp"),
            P("fs", "tp"),
            P(),
            P(),
            P(),
        ),
        out_specs=(P("grp", "tp"), P("grp", "tp"), P("grp", "tp"), P(("grp", "fs", "tp"), None)),
        check_vma=False,
    )
```

time: 187 us -> 115 us (0.61); the launches traced: 183 us -> 115 us
  Pallas kernels: 0 us -> 114 us
  waiting for transfers between devices: 101 us -> 0 us
  blocking collectives: 36.6 us -> 0 us
  between operations: 14.1 us -> 0.64 us
  local copies, waits for them, and re-layouts: 13.2 us -> 0 us
  matrix products: 9.08 us -> 0 us
  other arithmetic: 8.29 us -> 0 us
    pallas_call x0 -> x2, Pallas kernels: none -> 114 us  [the longest x1 111 us: local(): pl.pallas_call(functools.partial(gather_and_reduce, n_fs, n_tp, units), o...]
    all_gather x1 -> x0, waiting for transfers between devices: 72.5 us -> none  [sent_together(): whole = lax.all_gather(both, axis, axis=dim, tiled=True)]
    all_to_all x1 -> x0, blocking collectives: 36.6 us -> none  [copy_for_each(): lax.all_to_all(jnp.broadcast_to(value[None], (devices, *value.shape)), ax...]
    reduce_scatter x1 -> x0, waiting for transfers between devices: 28.9 us -> none  [local(): lax.psum_scatter(lax.dot_general(hidden, down_ready, (((1,), (1,)), ((),...]
    dot_general x2 -> x0, matrix products: 9.08 us -> none  [the longest x1 6.74 us: local(): lax.dot_general(hidden, down_ready, (((1,), (1,)), ((), ())), preferred_e...]
    split x1 -> x0, local copies, waits for them, and re-layouts: 5.77 us -> none  [sent_together(): jnp.split(whole, [sum(widths[:k]) for k in range(1, len(widths))], axis=a...]
    unnamed x9 -> x0, local copies, waits for them, and re-layouts: 5.68 us -> none
    convert_element_type x4 -> x0, other arithmetic: 4.83 us -> none  [the longest x1 1.84 us: finish(): ((mixed - center) * lax.rsqrt(spread + 1e-05) * post_gain + post_bias).as...]
  transfers between devices with their start and end apart: 2 -> 0, of which waited for: 2 -> 0; matrix products, arithmetic and copies ran while one was open for 8% -> 0% of each run, Pallas kernels for 0% -> 0%
where the time goes in v2:
time: 115 us
  Pallas kernels  114 us (99%)
    pallas_call x1, Pallas kernels, local(): pl.pallas_call(functools.partial(gather_and_reduce, n_fs, n_tp, units), o...  111 us
    pallas_call x1, Pallas kernels, local(): pl.pallas_call(functools.partial(finish, units), out_shape=(pltpu.HBM((un...  3.16 us

profile of v2, /device:TPU:65, one launch (start us, length us, event | category | flops | bytes accessed | tf_op | source)
XLA Modules:
  0.0 114.6 jit_solution(4512297156141836388)
XLA Ops:
  0.6 110.8 %shard_map.102 = (bf16[16,3,352,128]{3,2,1,0:T(8,128)(2,1)S(1)}, f32[64,2048]{1,0:T(8,128)S(1)}, f32[2,1,2048]{2,1,0:T(1,128)S(1)}) custom-call(bf16[64,2048]{1,0:T(8,128)(2,1)} %tokens.1, f32[64,344]{1,0:T(8,128)} %gate.1, f32[64,344]{1,0:T(8,128)} %up.1, f32[64,344]{1,0:T(8,128)} %down.1, f32[16,128]{1,0:T(8,128)} %bitcast.6, f32[1,2048]{1,0:T(1,128)} %bitcast.7, ...), custom_call_target="tpu_custom_call" | custom-call | tf_op jit(solution)/shard_map/pallas_call | solution.py:388
  111.4 3.2 %shard_map.103 = (bf16[344,2048]{1,0:T(8,128)(2,1)}, bf16[344,2048]{1,0:T(8,128)(2,1)}, bf16[344,2048]{1,0:T(8,128)(2,1)}, bf16[64,2048]{1,0:T(8,128)(2,1)}) custom-call(bf16[16,3,352,128]{3,2,1,0:T(8,128)(2,1)S(1)} %get-tuple-element.11.ready, f32[64,2048]{1,0:T(8,128)S(1)} %get-tuple-element.12.mixed, f32[2,1,2048]{2,1,0:T(1,128)S(1)} %get-tuple-element.13.affine), custom_call_target="tpu_custom_call" | custom-call | tf_op jit(solution)/shard_map/pallas_call | solution.py:428

commit v3 on v2

--- a/solution.py
+++ b/solution.py
@@ -9,7 +9,8 @@
 
 MESH = pl.DeviceIdType.MESH
 CUTS = 8
-TOP = 8
+TOP = 7
+HUB = 2
 PARTS = 3
 VMEM_SPACE = pl.BlockSpec(memory_space=pltpu.VMEM)
 HBM_SPACE = pl.BlockSpec(memory_space=pltpu.HBM)
@@ -19,7 +20,7 @@
     n_fs, n_tp, units, tokens, gate, up, down, gain, post_gain, post_bias, ready, mixed, affine,
     tok_in, w_in, gain_in, normed, partial, sent, landed,
     in_sem, swap_sem, a_recv, a_send, b_recv, b_send, c_recv, c_send, core_recv, core_send,
-    x_recv, x_send, r_recv, r_send, first_in,
+    x_recv, x_send, r_recv, r_send, first_in, c_left,
 ):
     f, t = lax.axis_index("fs"), lax.axis_index("tp")
     nz = n_fs // 2
@@ -61,7 +62,12 @@
 
     @pl.when(z == 0)
     def _():
-        for i in range(TOP):
+        for i in range(HUB, TOP):
+            greet(fs=c + 2 * (low + i))
+
+    @pl.when(z == 1)
+    def _():
+        for i in range(HUB):
             greet(fs=c + 2 * (low + i))
 
     my_rows = pl.ds(pl.multiple_of(c * piece, piece), piece)
@@ -139,20 +145,24 @@
         ref = part(i, index)
         return remote(ref, ref, c_send.at[j], c_recv.at[j, i], fs=there)
 
+    def c_left_copy(i, j, index):
+        ref = part(i, index)
+        return remote(ref, ref, c_left.at[j], c_recv.at[j, i], fs=f - 2)
+
     def core_copy(i, index):
         ref = part(i, index)
         return remote(ref, ref, core_send.at[i], core_recv.at[i], fs=other)
 
     goes_right = z < nz - 1
-    goes_left = (z > 1) & (z != low)
+    goes_left = (z > 0) & (z != low)
     passes_top = z < low - 1
 
     @pl.when(z >= low)
     def _():
         for i in range(PARTS):
-            c_copy(i, z - low, z, c).start()
-
-    @pl.when(goes_left)
+            c_copy(i, z - low, z, jnp.where(z - low < HUB, 2, 0) + c).start()
+
+    @pl.when(goes_left & (z > 1))
     def _():
         for i in range(PARTS):
             b_copy(i, 1, z).start()
@@ -171,42 +181,42 @@
         for d in range(2):
             x_copy(d, 0, k).start()
 
+    @pl.when(z == 1)
+    def _():
+        pl.semaphore_wait(first_in, 1)
+        for i in range(PARTS):
+            b_copy(i, 1, z).start()
+
     left_most = max(low, TOP) - 1
     last_left = jnp.where(z < low, low - 1, nz - 1)
     events = []
     for j in range(1, nz - 1):
-        events.append((2.0 + 2.83 * j, "a", j))
+        events.append((5.0 + 3.0 * j, "a", j))
     for j in range(1, left_most + 1):
-        events.append((3.0 + 5.2 * j, "b", j))
+        events.append((10.0 + 6.0 * j, "b", j))
     for j in range(TOP):
-        events.append((2.0 * low + 18.0 + 2.83 * j, "c", j))
-    events.append((16.0, "x", 0))
-    events.append((2.0 * low + 17.0, "first", 0))
-    events.append((3.1 + 5.2 * (low - 2), "zero", 0))
-    for j in range(1, low):
-        events.append((1000.0 + j, "end", j))
+        events.append((2.0 * low + 27.0 + 2.4 * j, "c", j))
+    events.append((27.0, "x", 0))
+    events.append((2.0 * low + 33.5, "first", 0))
+    events.append((1000.0, "end", 0))
     for _, kind, j in sorted(events):
         if kind == "x":
             for d in range(2):
                 x_copy(d, 0, 2).wait_recv()
                 for k in (far, 3):
                     x_copy(d, 2, k).start()
-        if kind == "zero":
-
-            @pl.when(z == 1)
-            def _():
-                pl.semaphore_wait(first_in, 1)
-                for q in range(1, low):
-                    for i in range(PARTS):
-                        b_copy(i, q, q).start()
-
         if kind == "end":
 
             @pl.when(z == 0)
             def _():
-                for i in range(PARTS):
-                    b_copy(i, j, j).wait_recv()
-                    core_copy(i, j).start()
+                for j in range(1, low):
+                    for i in range(PARTS):
+                        b_copy(i, j, j).wait_recv()
+                        core_copy(i, j).start()
+                for j in range(HUB):
+                    for i in range(PARTS):
+                        c_copy(i, j, low + j, c).wait_recv()
+                        core_copy(i, low + j).start()
 
         if kind == "first":
 
@@ -249,10 +259,15 @@
 
         if kind == "c":
 
-            @pl.when(z < low)
+            @pl.when((z < low) if j >= HUB else (z > 0) & (z < low))
             def _():
                 for i in range(PARTS):
                     c_copy(i, j, low + j, c).wait_recv()
+                    if j < HUB:
+
+                        @pl.when(z == 1)
+                        def _():
+                            c_left_copy(i, j, low + j).start()
 
                     @pl.when(passes_top)
                     def _():
@@ -336,15 +351,22 @@
 
     for j in range(1, left_most + 1):
 
-        @pl.when((goes_left | (z == 1)) & (z + j - 1 <= last_left))
+        @pl.when(goes_left & (z + j - 1 <= last_left))
         def _():
             left(b_send.at[j - 1])
 
     for j in range(TOP):
 
-        @pl.when(passes_top | (z == low + j))
+        passes = passes_top if j >= HUB else passes_top & (z > 0)
+
+        @pl.when(passes | (z == low + j))
         def _():
             left(c_send.at[j])
+
+    @pl.when(z == 1)
+    def _():
+        for j in range(HUB):
+            left(c_left.at[j])
 
     for i in range(PARTS):
         ref = ready.at[all_others, 0, pl.ds(0, share), :]
@@ -417,6 +439,7 @@
             dma((2, far, CUTS)),
             dma((2, 2)),
             pltpu.SemaphoreType.REGULAR,
+            dma((HUB,)),
         ],
         compiler_params=pltpu.CompilerParams(
             collective_id=0, has_side_effects=True, vmem_limit_bytes=58 * 1024 * 1024

time: 115 us -> 104 us (0.904)
  Pallas kernels: 114 us -> 102 us
    pallas_call x1, Pallas kernels: 111 us -> 99 us  [local(): pl.pallas_call(functools.partial(gather_and_reduce, n_fs, n_tp, units), o...]
where the time goes in v3:
time: 104 us; the launch traced here: 103 us
  Pallas kernels  102 us (98%)
    pallas_call x1, Pallas kernels, local(): pl.pallas_call(functools.partial(gather_and_reduce, n_fs, n_tp, units), o...  99 us
    pallas_call x1, Pallas kernels, local(): pl.pallas_call(functools.partial(finish, units), out_shape=(pltpu.HBM((un...  3.16 us

profile of v3, /device:TPU:65, one launch (start us, length us, event | category | flops | bytes accessed | tf_op | source)
XLA Modules:
  0.0 102.8 jit_solution(47381673390057402)
XLA Ops:
  0.6 99.0 %shard_map.102 = (bf16[16,3,352,128]{3,2,1,0:T(8,128)(2,1)S(1)}, f32[64,2048]{1,0:T(8,128)S(1)}, f32[2,1,2048]{2,1,0:T(1,128)S(1)}) custom-call(bf16[64,2048]{1,0:T(8,128)(2,1)} %tokens.1, f32[64,344]{1,0:T(8,128)} %gate.1, f32[64,344]{1,0:T(8,128)} %up.1, f32[64,344]{1,0:T(8,128)} %down.1, f32[16,128]{1,0:T(8,128)} %bitcast.6, f32[1,2048]{1,0:T(1,128)} %bitcast.7, ...), custom_call_target="tpu_custom_call" | custom-call | tf_op jit(solution)/shard_map/pallas_call | solution.py:410
  99.6 3.2 %shard_map.103 = (bf16[344,2048]{1,0:T(8,128)(2,1)}, bf16[344,2048]{1,0:T(8,128)(2,1)}, bf16[344,2048]{1,0:T(8,128)(2,1)}, bf16[64,2048]{1,0:T(8,128)(2,1)}) custom-call(bf16[16,3,352,128]{3,2,1,0:T(8,128)(2,1)S(1)} %get-tuple-element.11.ready, f32[64,2048]{1,0:T(8,128)S(1)} %get-tuple-element.12.mixed, f32[2,1,2048]{2,1,0:T(1,128)S(1)} %get-tuple-element.13.affine), custom_call_target="tpu_custom_call" | custom-call | tf_op jit(solution)/shard_map/pallas_call | solution.py:451

commit v4 on v3

--- a/solution.py
+++ b/solution.py
@@ -300,10 +300,16 @@
             g = g_more if j == 0 else g + g_more
             u = u_more if j == 0 else u + u_more
         h = (g * (1.0 / (1.0 + jnp.exp(-g))) * u).astype(jnp.bfloat16)
-        for j in range(CUTS):
-            partial[j, rows, :] = jnp.dot(
-                h, cut_of(2, j), preferred_element_type=jnp.float32
-            ).astype(jnp.bfloat16)
+        done = set()
+
+        def ensure(j):
+            if j not in done:
+                done.add(j)
+                partial[j, rows, :] = jnp.dot(
+                    h, cut_of(2, j), preferred_element_type=jnp.float32
+                ).astype(jnp.bfloat16)
+
+        return ensure
 
     def r_copy(d, s, j):
         return remote(
@@ -314,10 +320,11 @@
     side = CUTS // 2
     for s in range(far):
         k = far - s
-        compute(k)
+        ensure = compute(k)
         for at in range(side if s == 0 else CUTS):
             for d in range(2):
                 j = d * side + at if s == 0 else ((1 - d) * side + at) % CUTS
+                ensure(j)
                 value = partial[j, pl.ds(slot(1 - d, k), block), :]
                 if s > 0 and not (s == 1 and j // side != d):
                     r_copy(d, s - 1, j).wait_recv()

time: 104 us -> 104 us (level)
  no operation moved by 1% of the time
where the time goes in v4:
time: 104 us; the launch traced here: 103 us
  Pallas kernels  102 us (98%)
    pallas_call x1, Pallas kernels, local(): pl.pallas_call(functools.partial(gather_and_reduce, n_fs, n_tp, units), o...  98.9 us
    pallas_call x1, Pallas kernels, local(): pl.pallas_call(functools.partial(finish, units), out_shape=(pltpu.HBM((un...  3.16 us

profile of v4, /device:TPU:65, one launch (start us, length us, event | category | flops | bytes accessed | tf_op | source)
XLA Modules:
  0.0 102.7 jit_solution(14096067584938204486)
XLA Ops:
  0.6 98.9 %shard_map.102 = (bf16[16,3,352,128]{3,2,1,0:T(8,128)(2,1)S(1)}, f32[64,2048]{1,0:T(8,128)S(1)}, f32[2,1,2048]{2,1,0:T(1,128)S(1)}) custom-call(bf16[64,2048]{1,0:T(8,128)(2,1)} %tokens.1, f32[64,344]{1,0:T(8,128)} %gate.1, f32[64,344]{1,0:T(8,128)} %up.1, f32[64,344]{1,0:T(8,128)} %down.1, f32[16,128]{1,0:T(8,128)} %bitcast.6, f32[1,2048]{1,0:T(1,128)} %bitcast.7, ...), custom_call_target="tpu_custom_call" | custom-call | tf_op jit(solution)/shard_map/pallas_call | solution.py:417
  99.6 3.2 %shard_map.103 = (bf16[344,2048]{1,0:T(8,128)(2,1)}, bf16[344,2048]{1,0:T(8,128)(2,1)}, bf16[344,2048]{1,0:T(8,128)(2,1)}, bf16[64,2048]{1,0:T(8,128)(2,1)}) custom-call(bf16[16,3,352,128]{3,2,1,0:T(8,128)(2,1)S(1)} %get-tuple-element.11.ready, f32[64,2048]{1,0:T(8,128)S(1)} %get-tuple-element.12.mixed, f32[2,1,2048]{2,1,0:T(1,128)S(1)} %get-tuple-element.13.affine), custom_call_target="tpu_custom_call" | custom-call | tf_op jit(solution)/shard_map/pallas_call | solution.py:458
